TPU v7x, 128 devices: a whole 4x4x4 slice. The times are simulated.
128 devices in a mesh: ra: 16 (over z, x), cb: 8 (over y, core).
Axes of the slice: x: 4, y: 4, z: 4, core: 2. Of those that a mesh axis runs over, the one named last changes fastest.
Arguments:
- inputs: bfloat16 [1536, 4096], P(None, 'ra'), may hold values from -12 to 12
- gate_weight: bfloat16 [2, 4096, 11264], P(None, 'ra', 'cb'), may hold values from -0.09375 to 0.09375
- up_weight: bfloat16 [2, 4096, 11264], P(None, 'ra', 'cb'), may hold values from -0.09375 to 0.09375
- down_weight: bfloat16 [2, 11264, 4096], P(None, 'cb', 'ra'), may hold values from -0.0546875 to 0.0546875
- norm_gain: float32 [2, 4096], P(None, 'ra'), may hold values from 0.05 to 8
- norm_shift: float32 [2, 4096], P(None, 'ra'), may hold values from -1.5 to 1.5
Outputs:
- outputs: bfloat16 [1536, 4096], P(None, 'ra')
All inputs are finite; a program needn't handle non-finite values.
Results may differ from a plain program's by a relative error of at most 0.04.
Values may be sent and summed in bfloat16 or wider, within the bound.
No kernel may reach another device: no remote copies, remote signals or barrier semaphores. Data moves between devices by JAX's collectives and lax.ppermute only.
A program may use at most 64 MiB of HBM per device.

v0:
```python
import jax
import jax.numpy as jnp
from jax import lax
from jax.sharding import Mesh
from jax.sharding import PartitionSpec as P

RESIDUAL = 0.5
EPSILON = 1e-05
BF16 = jnp.bfloat16
F32 = jnp.float32


def exchange(parts, axes):
    return lax.all_to_all(parts, axes, 0, 0, tiled=True)


def share(block, axes, peers):
    return exchange(jnp.broadcast_to(block[None], (peers, *block.shape)), axes)


def swap_core(block):
    return lax.ppermute(block, "c", [(0, 1), (1, 0)])


def dot_nt(a, b):
    return lax.dot_general(a, b, (((1,), (1,)), ((), ())), preferred_element_type=F32)


def regroup_weights(gate, up, down):
    stacked = jnp.stack((gate.T, up.T, down))
    rows = stacked.shape[1] // 4
    parts = stacked.reshape(3, 4, rows, 256).transpose(1, 0, 2, 3)
    mine = exchange(parts, "x")
    mine = mine.transpose(1, 2, 0, 3).reshape(3, rows, 1024)
    other = swap_core(mine)
    both = jnp.concatenate((mine, other), axis=1)
    return (both[:2].reshape(2 * 2 * rows, 1024), both[2])


def normed(mixed, row_sum, row_squares, gain, shift):
    mean = row_sum / 4096.0
    var = row_squares / 4096.0 - mean * mean
    out = (mixed - mean[:, None]) * lax.rsqrt(var + EPSILON)[:, None]
    return (out * gain + shift).astype(BF16)


def hidden_units(stream, w_gu):
    partial = dot_nt(stream, w_gu).astype(BF16)
    cols = partial.shape[1] // 2
    summed = exchange(partial.reshape(4, -1, 2 * cols), "z").astype(F32).sum(axis=0)
    hidden = (jax.nn.silu(summed[:, :cols]) * summed[:, cols:]).astype(BF16)
    return share(hidden, "z", 4).reshape(-1, cols)


def per_device(inputs, gate_weight, up_weight, down_weight, norm_gain, norm_shift):
    c = lax.axis_index("c")
    x = lax.axis_index("x")
    y = lax.axis_index("y")
    half = inputs.shape[0] // 2
    quarter = half // 4
    mine = lax.dynamic_slice_in_dim(inputs, c * half + y * quarter, quarter, 0)
    rows = share(mine, "x", 4).transpose(1, 0, 2).reshape(quarter, 1024)
    stream = share(rows, "y", 4).reshape(half, 1024)
    affine = jnp.stack((norm_gain[0], norm_shift[0]))
    affine = lax.all_gather(affine, "x", axis=1, tiled=True)
    gu0, down0 = regroup_weights(gate_weight[0], up_weight[0], down_weight[0])
    gu1, down1 = regroup_weights(gate_weight[1], up_weight[1], down_weight[1])
    hidden = hidden_units(stream, gu0)
    partial = jnp.dot(hidden, down0, preferred_element_type=F32).astype(BF16)
    block = half // 16
    branch = exchange(partial.reshape(16, block, 1024), ("x", "y")).astype(F32).sum(axis=0)
    own = lax.dynamic_slice_in_dim(stream, (x * 4 + y) * block, block, 0)
    mixed = RESIDUAL * own.astype(F32) + branch
    stats = lax.psum(jnp.stack((mixed.sum(axis=1), (mixed * mixed).sum(axis=1))), "z")
    out = normed(mixed, stats[0], stats[1], affine[0], affine[1])
    stream = share(out, ("x", "y"), 16).reshape(half, 1024)
    hidden = hidden_units(stream, gu1)
    partial = jnp.dot(hidden, down1, preferred_element_type=F32).astype(BF16)
    parts = partial.reshape(4, quarter, 4, 256).transpose(2, 0, 1, 3).reshape(16, quarter, 256)
    branch = exchange(parts, ("x", "y")).astype(F32).sum(axis=0)
    own = lax.dynamic_slice(stream, (y * quarter, x * 256), (quarter, 256))
    mixed = RESIDUAL * own.astype(F32) + branch
    stats = lax.psum(jnp.stack((mixed.sum(axis=1), (mixed * mixed).sum(axis=1))), ("z", "x"))
    out = normed(mixed, stats[0], stats[1], norm_gain[1], norm_shift[1])
    ours = share(out, "y", 4).reshape(half, 256)
    theirs = swap_core(ours)
    result = jnp.concatenate((ours, theirs), axis=0)
    swapped = jnp.concatenate((theirs, ours), axis=0)
    return jnp.where(c == 0, result, swapped)


def solution(mesh):
    finer = Mesh(mesh.devices.reshape(4, 4, 4, 2), ("z", "x", "y", "c"))
    ra, cb = (("z", "x"), ("y", "c"))
    in_specs = (
        P(None, ra),
        P(None, ra, cb),
        P(None, ra, cb),
        P(None, cb, ra),
        P(None, ra),
        P(None, ra),
    )
    return jax.shard_map(
        per_device, mesh=finer, in_specs=in_specs, out_specs=P(None, ra), check_vma=False
    )
```

profile of v0, /device:TPU:1, one launch (start us, length us, event | category | flops | bytes accessed | tf_op | source)
XLA Modules:
  0.0 365.9 jit_solution(2115882943331297913)
XLA Ops:
  0.0 2.4 fusion.6
  2.7 2.3 fusion.7
  5.2 2.3 fusion.8
  7.9 30.5 %all_to_all.60 = bf16[4,3,352,256]{3,2,1,0:T(8,128)(2,1)S(1)} all-to-all(bf16[4,3,352,256]{3,2,1,0:T(8,128)(2,1)S(1)} %copy.30), channel_id=1, replica_groups=mesh['z'=4,'x'=4,'y'=4,'c'=2] {'x'}, dimensions={0} | all-to-all | bytes 4325376 | tf_op jit(solution)/shard_map/all_to_all | solution.py:14
  38.7 2.2 collective-permute-start
  41.0 10.2 %all_to_all.61 = bf16[4,192,256]{2,1,0:T(8,128)(2,1)S(1)} all-to-all(bf16[4,192,256]{2,1,0:T(8,128)(2,1)S(1)} %broadcast_in_dim.14), channel_id=1, replica_groups=mesh['z'=4,'x'=4,'y'=4,'c'=2] {'x'}, dimensions={0} | all-to-all | bytes 786432 | tf_op jit(solution)/shard_map/all_to_all | solution.py:14
  52.7 4.4 %all-to-all-start.1 = ((bf16[4,192,1024]{2,1,0:T(8,128)(2,1)}), bf16[4,192,1024]{2,1,0:T(8,128)(2,1)}, u32[]{:S(2)}, u32[]{:S(2)}) async-start(bf16[4,192,1024]{2,1,0:T(8,128)(2,1)} %broadcast_in_dim.16), calls=%async_computation.1 | async-start | bytes 3145728 | tf_op jit(solution)/shard_map/all_to_all | solution.py:14
  59.0 2.0 copy-done.2
  62.9 13.6 %all-to-all-done.1 = bf16[4,192,1024]{2,1,0:T(8,128)(2,1)} async-done(((bf16[4,192,1024]{2,1,0:T(8,128)(2,1)}), bf16[4,192,1024]{2,1,0:T(8,128)(2,1)}, u32[]{:S(2)}, u32[]{:S(2)}) %all-to-all-start.1) | async-done | bytes 1572896 | tf_op jit(solution)/shard_map/all_to_all | solution.py:14
  76.5 4.9 %convolution_convert_fusion.1 = bf16[768,1408]{1,0:T(8,128)(2,1)S(1)} fusion(bf16[768,1024]{1,0:T(8,128)(2,1)} %bitcast.1, bf16[1408,1024]{1,0:T(8,128)(2,1)} %bitcast.85), kind=kOutput, calls=%fused_computation.3 | convolution fusion | flops 2215673856 | bytes 6619136 | tf_op jit(solution)/shard_map/dot_general | solution.py:26
  81.5 29.2 %all_to_all.62 = bf16[4,192,1408]{2,1,0:T(8,128)(2,1)S(1)} all-to-all(bf16[4,192,1408]{2,1,0:T(8,128)(2,1)S(1)} %bitcast.93), channel_id=1, replica_groups=mesh['z'=4,'x'=4,'y'=4,'c'=2] {'z'}, dimensions={0} | all-to-all | bytes 4325376 | tf_op jit(solution)/shard_map/all_to_all | solution.py:14
  112.4 4.4 %all-to-all-start.4 = ((bf16[4,192,704]{2,1,0:T(8,128)(2,1)}), bf16[4,192,704]{2,1,0:T(8,128)(2,1)}, u32[]{:S(2)}, u32[]{:S(2)}) async-start(bf16[4,192,704]{2,1,0:T(8,128)(2,1)} %broadcast_in_dim.17), calls=%async_computation.4 | async-start | bytes 2359296 | tf_op jit(solution)/shard_map/all_to_all | solution.py:14
  119.1 10.4 %all-to-all-done.4 = bf16[4,192,704]{2,1,0:T(8,128)(2,1)} async-done(((bf16[4,192,704]{2,1,0:T(8,128)(2,1)}), bf16[4,192,704]{2,1,0:T(8,128)(2,1)}, u32[]{:S(2)}, u32[]{:S(2)}) %all-to-all-start.4) | async-done | bytes 1081376 | tf_op jit(solution)/shard_map/all_to_all | solution.py:14
  129.5 3.6 all-to-all-start.7
  133.2 4.3 %convolution_convert_fusion.3 = bf16[768,1024]{1,0:T(8,128)(2,1)} fusion(bf16[768,704]{1,0:T(8,128)(2,1)} %bitcast.13, bf16[3,704,1024]{2,1,0:T(8,128)(2,1)} %copy-done.2), kind=kOutput, calls=%fused_computation.9 | convolution fusion | flops 1108082688 | bytes 4194304 | tf_op jit(solution)/shard_map/dot_general | solution.py:69
  137.5 18.0 %all-to-all-done.7 = bf16[4,3,352,256]{3,2,1,0:T(8,128)(2,1)S(1)} async-done(((bf16[4,3,352,256]{3,2,1,0:T(8,128)(2,1)}), bf16[4,3,352,256]{3,2,1,0:T(8,128)(2,1)S(1)}, u32[]{:S(2)}, u32[]{:S(2)}) %all-to-all-start.7) | async-done | bytes 2162720 | tf_op jit(solution)/shard_map/all_to_all | solution.py:14
  155.5 4.4 %all-to-all-start.5 = ((bf16[16,48,1024]{2,1,0:T(8,128)(2,1)}), bf16[16,48,1024]{2,1,0:T(8,128)(2,1)}, u32[]{:S(2)}, u32[]{:S(2)}) async-start(bf16[16,48,1024]{2,1,0:T(8,128)(2,1)} %bitcast.95), calls=%async_computation.5 | async-start | bytes 3145728 | tf_op jit(solution)/shard_map/all_to_all | solution.py:14
  160.0 18.8 %all_gather.3 = f32[2,1024]{1,0:T(2,128)S(1)} all-gather(f32[2,256]{1,0:T(2,128)S(1)} %pad_maximum_fusion), channel_id=1, replica_groups=mesh['z'=4,'x'=4,'y'=4,'c'=2] {'x'}, dimensions={1}, use_global_device_ids=true | all-gather | bytes 10240 | tf_op jit(solution)/shard_map/all_gather | solution.py:65
  180.4 8.3 %collective-permute-start.1 = (bf16[3,352,1024]{2,1,0:T(8,128)(2,1)}, bf16[3,352,1024]{2,1,0:T(8,128)(2,1)S(1)}, u32[]{:S(2)}, u32[]{:S(2)}) collective-permute-start(bf16[3,352,1024]{2,1,0:T(8,128)(2,1)} %bitcast.59), channel_id=1, source_target_pairs={{0,1},{1,0},{2,3},{3,2},{4,5},{5,4},{6,7},{7,6},{8,9},{9,8},{10,11... | collective-permute-start | bytes 6488072 | tf_op jit(solution)/shard_map/ppermute | solution.py:22
  191.5 6.9 %psum.14 = f32[2,48]{1,0:T(2,128)S(1)} all-reduce(f32[2,48]{1,0:T(2,128)S(1)} %pad_maximum_fusion.2), channel_id=1, replica_groups=mesh['z'=4,'x'=4,'y'=4,'c'=2] {'z'}, use_global_device_ids=true, to_apply=%region_4.5 | all-reduce | flops 96 | bytes 768 | tf_op jit(solution)/shard_map/psum | solution.py:74
  200.8 5.1 %all-to-all-start.6 = ((bf16[16,48,1024]{2,1,0:T(8,128)(2,1)}), bf16[16,48,1024]{2,1,0:T(8,128)(2,1)}, u32[]{:S(2)}, u32[]{:S(2)}) async-start(bf16[16,48,1024]{2,1,0:T(8,128)(2,1)} %broadcast_in_dim.18), calls=%async_computation.6 | async-start | bytes 3145728 | tf_op jit(solution)/shard_map/all_to_all | solution.py:14
  211.8 14.5 %all-to-all-done.6 = bf16[16,48,1024]{2,1,0:T(8,128)(2,1)} async-done(((bf16[16,48,1024]{2,1,0:T(8,128)(2,1)}), bf16[16,48,1024]{2,1,0:T(8,128)(2,1)}, u32[]{:S(2)}, u32[]{:S(2)}) %all-to-all-start.6) | async-done | bytes 1572896 | tf_op jit(solution)/shard_map/all_to_all | solution.py:14
  226.3 4.9 %convolution_convert_fusion = bf16[768,1408]{1,0:T(8,128)(2,1)S(1)} fusion(bf16[768,1024]{1,0:T(8,128)(2,1)} %bitcast.22, bf16[1408,1024]{1,0:T(8,128)(2,1)} %bitcast.86), kind=kOutput, calls=%fused_computation.2 | convolution fusion | flops 2215673856 | bytes 6619136 | tf_op jit(solution)/shard_map/dot_general | solution.py:26
  231.3 25.4 %all_to_all.63 = bf16[4,192,1408]{2,1,0:T(8,128)(2,1)S(1)} all-to-all(bf16[4,192,1408]{2,1,0:T(8,128)(2,1)S(1)} %bitcast.94), channel_id=1, replica_groups=mesh['z'=4,'x'=4,'y'=4,'c'=2] {'z'}, dimensions={0} | all-to-all | bytes 4325376 | tf_op jit(solution)/shard_map/all_to_all | solution.py:14
  257.4 13.7 %all_to_all.64 = bf16[4,192,704]{2,1,0:T(8,128)(2,1)S(1)} all-to-all(bf16[4,192,704]{2,1,0:T(8,128)(2,1)S(1)} %broadcast_in_dim.19), channel_id=1, replica_groups=mesh['z'=4,'x'=4,'y'=4,'c'=2] {'z'}, dimensions={0} | all-to-all | bytes 2162688 | tf_op jit(solution)/shard_map/all_to_all | solution.py:14
  271.1 3.9 %convolution_convert_fusion.2 = bf16[768,1024]{1,0:T(8,128)(2,1)} fusion(bf16[768,704]{1,0:T(8,128)(2,1)S(1)} %bitcast.100, bf16[3,704,1024]{2,1,0:T(8,128)(2,1)} %copy-done.3), kind=kOutput, calls=%fused_computation.8 | convolution fusion | flops 1108082688 | bytes 4096000 | tf_op jit(solution)/shard_map/dot_general | solution.py:78
  275.0 2.9 reshape.113
  279.3 10.2 %all-to-all-start.10 = ((bf16[16,192,256]{2,1,0:T(8,128)(2,1)}), bf16[16,192,256]{2,1,0:T(8,128)(2,1)S(1)}, u32[]{:S(2)}, u32[]{:S(2)}) async-start(bf16[16,192,256]{2,1,0:T(8,128)(2,1)} %bitcast.84), calls=%async_computation.10 | async-start | bytes 3145728 | tf_op jit(solution)/shard_map/all_to_all | solution.py:14
  289.6 19.0 %all-to-all-done.10 = bf16[16,192,256]{2,1,0:T(8,128)(2,1)S(1)} async-done(((bf16[16,192,256]{2,1,0:T(8,128)(2,1)}), bf16[16,192,256]{2,1,0:T(8,128)(2,1)S(1)}, u32[]{:S(2)}, u32[]{:S(2)}) %all-to-all-start.10) | async-done | bytes 1572896 | tf_op jit(solution)/shard_map/all_to_all | solution.py:14
  309.9 31.9 %psum.15 = f32[2,192]{1,0:T(2,128)S(1)} all-reduce(f32[2,192]{1,0:T(2,128)S(1)} %pad_maximum_fusion.1), channel_id=1, replica_groups=mesh['z'=4,'x'=4,'y'=4,'c'=2] {'z','x'}, use_global_device_ids=true, to_apply=%region_9.10 | all-reduce | flops 384 | bytes 3072 | tf_op jit(solution)/shard_map/psum | solution.py:83
  342.9 10.1 %all_to_all.65 = bf16[4,192,256]{2,1,0:T(8,128)(2,1)S(1)} all-to-all(bf16[4,192,256]{2,1,0:T(8,128)(2,1)S(1)} %broadcast_in_dim.20), channel_id=1, replica_groups=mesh['z'=4,'x'=4,'y'=4,'c'=2] {'y'}, dimensions={0} | all-to-all | bytes 786432 | tf_op jit(solution)/shard_map/all_to_all | solution.py:14
  353.0 10.3 %collective-permute-start.2 = (bf16[768,256]{1,0:T(8,128)(2,1)S(1)}, bf16[768,256]{1,0:T(8,128)(2,1)S(1)}, u32[]{:S(2)}, u32[]{:S(2)}) collective-permute-start(bf16[768,256]{1,0:T(8,128)(2,1)S(1)} %bitcast.97), channel_id=1, source_target_pairs={{0,1},{1,0},{2,3},{3,2},{4,5},{5,4},{6,7},{7,6},{8,9},{9,8},{10,11... | collective-permute-start | bytes 1179656 | tf_op jit(solution)/shard_map/ppermute | solution.py:22
  (66 shorter events, 30.2 us)
Async XLA Ops:
  0.0 40.9 %copy-start = (bf16[1536,256]{1,0:T(8,128)(2,1)S(1)}, bf16[1536,256]{1,0:T(8,128)(2,1)}, u32[]{:S(2)}) copy-start(bf16[1536,256]{1,0:T(8,128)(2,1)} %param.6) | copy-start | bytes 2359300
  38.7 18.5 %collective-permute-start = (bf16[3,352,1024]{2,1,0:T(8,128)(2,1)S(1)}, bf16[3,352,1024]{2,1,0:T(8,128)(2,1)}, u32[]{:S(2)}, u32[]{:S(2)}) collective-permute-start(bf16[3,352,1024]{2,1,0:T(8,128)(2,1)S(1)} %bitcast.81), channel_id=1, source_target_pairs={{0,1},{1,0},{2,3},{3,2},{4,5},{5,4},{6,7},{7,6},{8,9},{9,8},{10,11... | collective-permute-start | bytes 6488072 | tf_op jit(solution)/shard_map/ppermute | solution.py:22
  52.7 23.9 %all-to-all-start.1 = ((bf16[4,192,1024]{2,1,0:T(8,128)(2,1)}), bf16[4,192,1024]{2,1,0:T(8,128)(2,1)}, u32[]{:S(2)}, u32[]{:S(2)}) async-start(bf16[4,192,1024]{2,1,0:T(8,128)(2,1)} %broadcast_in_dim.16), calls=%async_computation.1 | async-start | bytes 3145728 | tf_op jit(solution)/shard_map/all_to_all | solution.py:14
  59.0 2.1 copy-start.2
  111.2 5.6 %copy-start.4 = (bf16[1,256,1408]{2,1,0:T(8,128)(2,1)S(1)}, bf16[1,256,1408]{2,1,0:T(8,128)(2,1)}, u32[]{:S(2)}) copy-start(bf16[1,256,1408]{2,1,0:T(8,128)(2,1)} %get-tuple-element.9) | copy-start | bytes 2162692
  112.4 4.7 %copy-start.5 = (bf16[1,256,1408]{2,1,0:T(8,128)(2,1)S(1)}, bf16[1,256,1408]{2,1,0:T(8,128)(2,1)}, u32[]{:S(2)}) copy-start(bf16[1,256,1408]{2,1,0:T(8,128)(2,1)} %get-tuple-element.11) | copy-start | bytes 2162692
  112.4 5.0 %copy-start.6 = (bf16[1,1408,256]{2,1,0:T(8,128)(2,1)S(1)}, bf16[1,1408,256]{2,1,0:T(8,128)(2,1)}, u32[]{:S(2)}) copy-start(bf16[1,1408,256]{2,1,0:T(8,128)(2,1)} %get-tuple-element.13) | copy-start | bytes 2162692
  112.4 17.1 %all-to-all-start.4 = ((bf16[4,192,704]{2,1,0:T(8,128)(2,1)}), bf16[4,192,704]{2,1,0:T(8,128)(2,1)}, u32[]{:S(2)}, u32[]{:S(2)}) async-start(bf16[4,192,704]{2,1,0:T(8,128)(2,1)} %broadcast_in_dim.17), calls=%async_computation.4 | async-start | bytes 2359296 | tf_op jit(solution)/shard_map/all_to_all | solution.py:14
  129.5 25.9 %all-to-all-start.7 = ((bf16[4,3,352,256]{3,2,1,0:T(8,128)(2,1)}), bf16[4,3,352,256]{3,2,1,0:T(8,128)(2,1)S(1)}, u32[]{:S(2)}, u32[]{:S(2)}) async-start(bf16[4,3,352,256]{3,2,1,0:T(8,128)(2,1)} %copy.34), calls=%async_computation.7 | async-start | bytes 4325376 | tf_op jit(solution)/shard_map/all_to_all | solution.py:14
  137.5 22.4 %copy-start.7 = (f32[2,256]{1,0:T(2,128)S(1)}, f32[2,256]{1,0:T(2,128)}, u32[]{:S(2)}) copy-start(f32[2,256]{1,0:T(2,128)} %param.10) | copy-start | bytes 6148
  137.5 22.5 %copy-start.8 = (f32[2,256]{1,0:T(2,128)S(1)}, f32[2,256]{1,0:T(2,128)}, u32[]{:S(2)}) copy-start(f32[2,256]{1,0:T(2,128)} %param.11) | copy-start | bytes 6148
  155.5 33.3 %all-to-all-start.5 = ((bf16[16,48,1024]{2,1,0:T(8,128)(2,1)}), bf16[16,48,1024]{2,1,0:T(8,128)(2,1)}, u32[]{:S(2)}, u32[]{:S(2)}) async-start(bf16[16,48,1024]{2,1,0:T(8,128)(2,1)} %bitcast.95), calls=%async_computation.5 | async-start | bytes 3145728 | tf_op jit(solution)/shard_map/all_to_all | solution.py:14
  180.4 27.2 %collective-permute-start.1 = (bf16[3,352,1024]{2,1,0:T(8,128)(2,1)}, bf16[3,352,1024]{2,1,0:T(8,128)(2,1)S(1)}, u32[]{:S(2)}, u32[]{:S(2)}) collective-permute-start(bf16[3,352,1024]{2,1,0:T(8,128)(2,1)} %bitcast.59), channel_id=1, source_target_pairs={{0,1},{1,0},{2,3},{3,2},{4,5},{5,4},{6,7},{7,6},{8,9},{9,8},{10,11... | collective-permute-start | bytes 6488072 | tf_op jit(solution)/shard_map/ppermute | solution.py:22
  200.8 25.5 %all-to-all-start.6 = ((bf16[16,48,1024]{2,1,0:T(8,128)(2,1)}), bf16[16,48,1024]{2,1,0:T(8,128)(2,1)}, u32[]{:S(2)}, u32[]{:S(2)}) async-start(bf16[16,48,1024]{2,1,0:T(8,128)(2,1)} %broadcast_in_dim.18), calls=%async_computation.6 | async-start | bytes 3145728 | tf_op jit(solution)/shard_map/all_to_all | solution.py:14
  207.9 2.0 copy-start.3
  279.3 29.2 %all-to-all-start.10 = ((bf16[16,192,256]{2,1,0:T(8,128)(2,1)}), bf16[16,192,256]{2,1,0:T(8,128)(2,1)S(1)}, u32[]{:S(2)}, u32[]{:S(2)}) async-start(bf16[16,192,256]{2,1,0:T(8,128)(2,1)} %bitcast.84), calls=%async_computation.10 | async-start | bytes 3145728 | tf_op jit(solution)/shard_map/all_to_all | solution.py:14
  308.6 57.3 %copy-start.1 = (bf16[1536,256]{1,0:T(8,128)(2,1)S(1)}, bf16[1536,256]{1,0:T(8,128)(2,1)}, u32[]{:S(2)}) copy-start(bf16[1536,256]{1,0:T(8,128)(2,1)} %param.6) | copy-start | bytes 2359300
  353.0 11.7 %collective-permute-start.2 = (bf16[768,256]{1,0:T(8,128)(2,1)S(1)}, bf16[768,256]{1,0:T(8,128)(2,1)S(1)}, u32[]{:S(2)}, u32[]{:S(2)}) collective-permute-start(bf16[768,256]{1,0:T(8,128)(2,1)S(1)} %bitcast.97), channel_id=1, source_target_pairs={{0,1},{1,0},{2,3},{3,2},{4,5},{5,4},{6,7},{7,6},{8,9},{9,8},{10,11... | collective-permute-start | bytes 1179656 | tf_op jit(solution)/shard_map/ppermute | solution.py:22
where the time goes:
time: 367 us; the launch traced here: 366 us
  blocking collectives  177 us (48%)
  waiting for transfers between devices  76.9 us (21%)
  starting transfers between devices  52.9 us (14%)
  local copies, waits for them, and re-layouts  31.9 us (9%)
  matrix products  18.1 us (5%)
  other arithmetic  8.87 us (2%)
    all_to_all x6, blocking collectives, exchange(): return lax.all_to_all(parts, axes, 0, 0, tiled=True)  119 us
    all_to_all x6, waiting for transfers between devices, exchange(): return lax.all_to_all(parts, axes, 0, 0, tiled=True)  75.6 us
    all_to_all x6, starting transfers between devices, exchange(): return lax.all_to_all(parts, axes, 0, 0, tiled=True)  32.1 us
    psum x1, blocking collectives, per_device(): lax.psum(jnp.stack((mixed.sum(axis=1), (mixed * mixed).sum(axis=1))), ('z...  31.9 us
    ppermute x3, starting transfers between devices, swap_core(): return lax.ppermute(block, 'c', [(0, 1), (1, 0)])  20.8 us
    all_gather x1, blocking collectives, per_device(): affine = lax.all_gather(affine, 'x', axis=1, tiled=True)  18.8 us
    dot_general x2, matrix products, dot_nt(): lax.dot_general(a, b, (((1,), (1,)), ((), ())), preferred_element_type=F32)  9.85 us
  transfers between devices with their start and end apart: 9, of which 6 were waited for; matrix products, arithmetic and copies ran while one was open for 6% of the time, Pallas kernels for 0%

commit v1 on v0

--- a/solution.py
+++ b/solution.py
@@ -80,7 +80,9 @@
     branch = exchange(parts, ("x", "y")).astype(F32).sum(axis=0)
     own = lax.dynamic_slice(stream, (y * quarter, x * 256), (quarter, 256))
     mixed = RESIDUAL * own.astype(F32) + branch
-    stats = lax.psum(jnp.stack((mixed.sum(axis=1), (mixed * mixed).sum(axis=1))), ("z", "x"))
+    stats = jnp.stack((mixed.sum(axis=1), (mixed * mixed).sum(axis=1)))
+    for name in ("x", "z"):
+        stats = lax.psum(stats, name)
     out = normed(mixed, stats[0], stats[1], norm_gain[1], norm_shift[1])
     ours = share(out, "y", 4).reshape(half, 256)
     theirs = swap_core(ours)

time: 367 us -> 348 us (0.948)
  blocking collectives: 177 us -> 160 us
    psum x1 -> x2, blocking collectives: 31.9 us -> 15.7 us  [per_device(): stats = lax.psum(stats, name)]
  transfers between devices with their start and end apart: 9 -> 9, of which waited for: 6 -> 6; matrix products, arithmetic and copies ran while one was open for 6% -> 7% of each run, Pallas kernels for 0% -> 0%
where the time goes in v1:
time: 348 us; the launch traced here: 346 us
  blocking collectives  160 us (46%)
  waiting for transfers between devices  76.8 us (22%)
  starting transfers between devices  49.9 us (14%)
  local copies, waits for them, and re-layouts  31.9 us (9%)
  matrix products  18.1 us (5%)
  other arithmetic  8.87 us (3%)
    all_to_all x6, blocking collectives, exchange(): return lax.all_to_all(parts, axes, 0, 0, tiled=True)  119 us
    all_to_all x6, waiting for transfers between devices, exchange(): return lax.all_to_all(parts, axes, 0, 0, tiled=True)  75.4 us
    all_to_all x6, starting transfers between devices, exchange(): return lax.all_to_all(parts, axes, 0, 0, tiled=True)  32 us
    all_gather x1, blocking collectives, per_device(): affine = lax.all_gather(affine, 'x', axis=1, tiled=True)  18.8 us
    ppermute x3, starting transfers between devices, swap_core(): return lax.ppermute(block, 'c', [(0, 1), (1, 0)])  17.9 us
    psum x2, blocking collectives, per_device(): stats = lax.psum(stats, name)  15.7 us
    dot_general x2, matrix products, dot_nt(): lax.dot_general(a, b, (((1,), (1,)), ((), ())), preferred_element_type=F32)  9.85 us
    unnamed x24, local copies, waits for them, and re-layouts  7.21 us
  transfers between devices with their start and end apart: 9, of which 6 were waited for; matrix products, arithmetic and copies ran while one was open for 7% of the time, Pallas kernels for 0%

profile of v1, /device:TPU:1, one launch (start us, length us, event | category | flops | bytes accessed | tf_op | source)
XLA Modules:
  0.0 346.3 jit_solution(16271070420660406616)
XLA Ops:
  0.0 2.4 fusion.6
  2.6 2.3 fusion.7
  5.2 2.3 fusion.8
  7.9 30.5 %all_to_all.60 = bf16[4,3,352,256]{3,2,1,0:T(8,128)(2,1)S(1)} all-to-all(bf16[4,3,352,256]{3,2,1,0:T(8,128)(2,1)S(1)} %copy.30), channel_id=1, replica_groups=mesh['z'=4,'x'=4,'y'=4,'c'=2] {'x'}, dimensions={0} | all-to-all | bytes 4325376 | tf_op jit(solution)/shard_map/all_to_all | solution.py:14
  38.7 2.2 collective-permute-start
  40.9 10.2 %all_to_all.61 = bf16[4,192,256]{2,1,0:T(8,128)(2,1)S(1)} all-to-all(bf16[4,192,256]{2,1,0:T(8,128)(2,1)S(1)} %broadcast_in_dim.14), channel_id=1, replica_groups=mesh['z'=4,'x'=4,'y'=4,'c'=2] {'x'}, dimensions={0} | all-to-all | bytes 786432 | tf_op jit(solution)/shard_map/all_to_all | solution.py:14
  52.6 4.3 %all-to-all-start.1 = ((bf16[4,192,1024]{2,1,0:T(8,128)(2,1)}), bf16[4,192,1024]{2,1,0:T(8,128)(2,1)}, u32[]{:S(2)}, u32[]{:S(2)}) async-start(bf16[4,192,1024]{2,1,0:T(8,128)(2,1)} %broadcast_in_dim.16), calls=%async_computation.1 | async-start | bytes 3145728 | tf_op jit(solution)/shard_map/all_to_all | solution.py:14
  62.9 13.6 %all-to-all-done.1 = bf16[4,192,1024]{2,1,0:T(8,128)(2,1)} async-done(((bf16[4,192,1024]{2,1,0:T(8,128)(2,1)}), bf16[4,192,1024]{2,1,0:T(8,128)(2,1)}, u32[]{:S(2)}, u32[]{:S(2)}) %all-to-all-start.1) | async-done | bytes 1572896 | tf_op jit(solution)/shard_map/all_to_all | solution.py:14
  76.5 4.9 %convolution_convert_fusion.1 = bf16[768,1408]{1,0:T(8,128)(2,1)S(1)} fusion(bf16[768,1024]{1,0:T(8,128)(2,1)} %bitcast.1, bf16[1408,1024]{1,0:T(8,128)(2,1)} %bitcast.85), kind=kOutput, calls=%fused_computation.3 | convolution fusion | flops 2215673856 | bytes 6619136 | tf_op jit(solution)/shard_map/dot_general | solution.py:26
  81.4 29.2 %all_to_all.62 = bf16[4,192,1408]{2,1,0:T(8,128)(2,1)S(1)} all-to-all(bf16[4,192,1408]{2,1,0:T(8,128)(2,1)S(1)} %bitcast.93), channel_id=1, replica_groups=mesh['z'=4,'x'=4,'y'=4,'c'=2] {'z'}, dimensions={0} | all-to-all | bytes 4325376 | tf_op jit(solution)/shard_map/all_to_all | solution.py:14
  112.3 4.4 %all-to-all-start.4 = ((bf16[4,192,704]{2,1,0:T(8,128)(2,1)}), bf16[4,192,704]{2,1,0:T(8,128)(2,1)}, u32[]{:S(2)}, u32[]{:S(2)}) async-start(bf16[4,192,704]{2,1,0:T(8,128)(2,1)} %broadcast_in_dim.17), calls=%async_computation.4 | async-start | bytes 2359296 | tf_op jit(solution)/shard_map/all_to_all | solution.py:14
  119.1 10.4 %all-to-all-done.4 = bf16[4,192,704]{2,1,0:T(8,128)(2,1)} async-done(((bf16[4,192,704]{2,1,0:T(8,128)(2,1)}), bf16[4,192,704]{2,1,0:T(8,128)(2,1)}, u32[]{:S(2)}, u32[]{:S(2)}) %all-to-all-start.4) | async-done | bytes 1081376 | tf_op jit(solution)/shard_map/all_to_all | solution.py:14
  129.4 3.6 %all-to-all-start.7 = ((bf16[4,3,352,256]{3,2,1,0:T(8,128)(2,1)}), bf16[4,3,352,256]{3,2,1,0:T(8,128)(2,1)S(1)}, u32[]{:S(2)}, u32[]{:S(2)}) async-start(bf16[4,3,352,256]{3,2,1,0:T(8,128)(2,1)} %copy.34), calls=%async_computation.7 | async-start | bytes 4325376 | tf_op jit(solution)/shard_map/all_to_all | solution.py:14
  133.1 4.3 %convolution_convert_fusion.3 = bf16[768,1024]{1,0:T(8,128)(2,1)} fusion(bf16[768,704]{1,0:T(8,128)(2,1)} %bitcast.13, bf16[3,704,1024]{2,1,0:T(8,128)(2,1)} %copy-done.2), kind=kOutput, calls=%fused_computation.9 | convolution fusion | flops 1108082688 | bytes 4194304 | tf_op jit(solution)/shard_map/dot_general | solution.py:69
  137.4 18.0 %all-to-all-done.7 = bf16[4,3,352,256]{3,2,1,0:T(8,128)(2,1)S(1)} async-done(((bf16[4,3,352,256]{3,2,1,0:T(8,128)(2,1)}), bf16[4,3,352,256]{3,2,1,0:T(8,128)(2,1)S(1)}, u32[]{:S(2)}, u32[]{:S(2)}) %all-to-all-start.7) | async-done | bytes 2162720 | tf_op jit(solution)/shard_map/all_to_all | solution.py:14
  155.3 4.4 %all-to-all-start.5 = ((bf16[16,48,1024]{2,1,0:T(8,128)(2,1)}), bf16[16,48,1024]{2,1,0:T(8,128)(2,1)}, u32[]{:S(2)}, u32[]{:S(2)}) async-start(bf16[16,48,1024]{2,1,0:T(8,128)(2,1)} %bitcast.95), calls=%async_computation.5 | async-start | bytes 3145728 | tf_op jit(solution)/shard_map/all_to_all | solution.py:14
  159.8 18.8 %all_gather.3 = f32[2,1024]{1,0:T(2,128)S(1)} all-gather(f32[2,256]{1,0:T(2,128)S(1)} %pad_maximum_fusion), channel_id=1, replica_groups=mesh['z'=4,'x'=4,'y'=4,'c'=2] {'x'}, dimensions={1}, use_global_device_ids=true | all-gather | bytes 10240 | tf_op jit(solution)/shard_map/all_gather | solution.py:65
  180.3 8.3 %collective-permute-start.1 = (bf16[3,352,1024]{2,1,0:T(8,128)(2,1)}, bf16[3,352,1024]{2,1,0:T(8,128)(2,1)S(1)}, u32[]{:S(2)}, u32[]{:S(2)}) collective-permute-start(bf16[3,352,1024]{2,1,0:T(8,128)(2,1)} %bitcast.59), channel_id=1, source_target_pairs={{0,1},{1,0},{2,3},{3,2},{4,5},{5,4},{6,7},{7,6},{8,9},{9,8},{10,11... | collective-permute-start | bytes 6488072 | tf_op jit(solution)/shard_map/ppermute | solution.py:22
  191.4 6.9 %psum.21 = f32[2,48]{1,0:T(2,128)S(1)} all-reduce(f32[2,48]{1,0:T(2,128)S(1)} %pad_maximum_fusion.2), channel_id=1, replica_groups=mesh['z'=4,'x'=4,'y'=4,'c'=2] {'z'}, use_global_device_ids=true, to_apply=%region_4.5 | all-reduce | flops 96 | bytes 768 | tf_op jit(solution)/shard_map/psum | solution.py:74
  200.7 5.1 %all-to-all-start.6 = ((bf16[16,48,1024]{2,1,0:T(8,128)(2,1)}), bf16[16,48,1024]{2,1,0:T(8,128)(2,1)}, u32[]{:S(2)}, u32[]{:S(2)}) async-start(bf16[16,48,1024]{2,1,0:T(8,128)(2,1)} %broadcast_in_dim.18), calls=%async_computation.6 | async-start | bytes 3145728 | tf_op jit(solution)/shard_map/all_to_all | solution.py:14
  211.7 14.5 %all-to-all-done.6 = bf16[16,48,1024]{2,1,0:T(8,128)(2,1)} async-done(((bf16[16,48,1024]{2,1,0:T(8,128)(2,1)}), bf16[16,48,1024]{2,1,0:T(8,128)(2,1)}, u32[]{:S(2)}, u32[]{:S(2)}) %all-to-all-start.6) | async-done | bytes 1572896 | tf_op jit(solution)/shard_map/all_to_all | solution.py:14
  226.2 4.9 %convolution_convert_fusion = bf16[768,1408]{1,0:T(8,128)(2,1)S(1)} fusion(bf16[768,1024]{1,0:T(8,128)(2,1)} %bitcast.22, bf16[1408,1024]{1,0:T(8,128)(2,1)} %bitcast.86), kind=kOutput, calls=%fused_computation.2 | convolution fusion | flops 2215673856 | bytes 6619136 | tf_op jit(solution)/shard_map/dot_general | solution.py:26
  231.1 25.4 %all_to_all.63 = bf16[4,192,1408]{2,1,0:T(8,128)(2,1)S(1)} all-to-all(bf16[4,192,1408]{2,1,0:T(8,128)(2,1)S(1)} %bitcast.94), channel_id=1, replica_groups=mesh['z'=4,'x'=4,'y'=4,'c'=2] {'z'}, dimensions={0} | all-to-all | bytes 4325376 | tf_op jit(solution)/shard_map/all_to_all | solution.py:14
  257.2 13.7 %all_to_all.64 = bf16[4,192,704]{2,1,0:T(8,128)(2,1)S(1)} all-to-all(bf16[4,192,704]{2,1,0:T(8,128)(2,1)S(1)} %broadcast_in_dim.19), channel_id=1, replica_groups=mesh['z'=4,'x'=4,'y'=4,'c'=2] {'z'}, dimensions={0} | all-to-all | bytes 2162688 | tf_op jit(solution)/shard_map/all_to_all | solution.py:14
  271.0 3.9 %convolution_convert_fusion.2 = bf16[768,1024]{1,0:T(8,128)(2,1)} fusion(bf16[768,704]{1,0:T(8,128)(2,1)S(1)} %bitcast.100, bf16[3,704,1024]{2,1,0:T(8,128)(2,1)} %copy-done.3), kind=kOutput, calls=%fused_computation.8 | convolution fusion | flops 1108082688 | bytes 4096000 | tf_op jit(solution)/shard_map/dot_general | solution.py:78
  274.9 2.9 reshape.113
  279.2 10.2 %all-to-all-start.10 = ((bf16[16,192,256]{2,1,0:T(8,128)(2,1)}), bf16[16,192,256]{2,1,0:T(8,128)(2,1)S(1)}, u32[]{:S(2)}, u32[]{:S(2)}) async-start(bf16[16,192,256]{2,1,0:T(8,128)(2,1)} %bitcast.84), calls=%async_computation.10 | async-start | bytes 3145728 | tf_op jit(solution)/shard_map/all_to_all | solution.py:14
  289.4 19.0 %all-to-all-done.10 = bf16[16,192,256]{2,1,0:T(8,128)(2,1)S(1)} async-done(((bf16[16,192,256]{2,1,0:T(8,128)(2,1)}), bf16[16,192,256]{2,1,0:T(8,128)(2,1)S(1)}, u32[]{:S(2)}, u32[]{:S(2)}) %all-to-all-start.10) | async-done | bytes 1572896 | tf_op jit(solution)/shard_map/all_to_all | solution.py:14
  309.8 8.8 %psum.22 = f32[2,192]{1,0:T(2,128)S(1)} all-reduce(f32[2,192]{1,0:T(2,128)S(1)} %pad_maximum_fusion.1), channel_id=1, replica_groups=mesh['z'=4,'x'=4,'y'=4,'c'=2] {'x'}, use_global_device_ids=true, to_apply=%region_9.10 | all-reduce | flops 384 | bytes 3072 | tf_op jit(solution)/shard_map/psum | solution.py:85
  318.6 6.9 %psum.23 = f32[2,192]{1,0:T(2,128)S(1)} all-reduce(f32[2,192]{1,0:T(2,128)S(1)} %psum.22), channel_id=1, replica_groups=mesh['z'=4,'x'=4,'y'=4,'c'=2] {'z'}, use_global_device_ids=true, to_apply=%region_10.11 | all-reduce | flops 384 | bytes 3072 | tf_op jit(solution)/shard_map/psum | solution.py:85
  326.5 9.8 %all_to_all.65 = bf16[4,192,256]{2,1,0:T(8,128)(2,1)S(1)} all-to-all(bf16[4,192,256]{2,1,0:T(8,128)(2,1)S(1)} %broadcast_in_dim.20), channel_id=1, replica_groups=mesh['z'=4,'x'=4,'y'=4,'c'=2] {'y'}, dimensions={0} | all-to-all | bytes 786432 | tf_op jit(solution)/shard_map/all_to_all | solution.py:14
  336.4 7.4 %collective-permute-start.2 = (bf16[768,256]{1,0:T(8,128)(2,1)S(1)}, bf16[768,256]{1,0:T(8,128)(2,1)S(1)}, u32[]{:S(2)}, u32[]{:S(2)}) collective-permute-start(bf16[768,256]{1,0:T(8,128)(2,1)S(1)} %bitcast.97), channel_id=1, source_target_pairs={{0,1},{1,0},{2,3},{3,2},{4,5},{5,4},{6,7},{7,6},{8,9},{9,8},{10,11... | collective-permute-start | bytes 1179656 | tf_op jit(solution)/shard_map/ppermute | solution.py:22
  (67 shorter events, 32.3 us)
Async XLA Ops:
  0.0 40.9 %copy-start = (bf16[1536,256]{1,0:T(8,128)(2,1)S(1)}, bf16[1536,256]{1,0:T(8,128)(2,1)}, u32[]{:S(2)}) copy-start(bf16[1536,256]{1,0:T(8,128)(2,1)} %param.6) | copy-start | bytes 2359300
  38.7 18.5 %collective-permute-start = (bf16[3,352,1024]{2,1,0:T(8,128)(2,1)S(1)}, bf16[3,352,1024]{2,1,0:T(8,128)(2,1)}, u32[]{:S(2)}, u32[]{:S(2)}) collective-permute-start(bf16[3,352,1024]{2,1,0:T(8,128)(2,1)S(1)} %bitcast.81), channel_id=1, source_target_pairs={{0,1},{1,0},{2,3},{3,2},{4,5},{5,4},{6,7},{7,6},{8,9},{9,8},{10,11... | collective-permute-start | bytes 6488072 | tf_op jit(solution)/shard_map/ppermute | solution.py:22
  52.6 23.8 %all-to-all-start.1 = ((bf16[4,192,1024]{2,1,0:T(8,128)(2,1)}), bf16[4,192,1024]{2,1,0:T(8,128)(2,1)}, u32[]{:S(2)}, u32[]{:S(2)}) async-start(bf16[4,192,1024]{2,1,0:T(8,128)(2,1)} %broadcast_in_dim.16), calls=%async_computation.1 | async-start | bytes 3145728 | tf_op jit(solution)/shard_map/all_to_all | solution.py:14
  59.0 2.1 copy-start.2
  111.1 5.6 %copy-start.4 = (bf16[1,256,1408]{2,1,0:T(8,128)(2,1)S(1)}, bf16[1,256,1408]{2,1,0:T(8,128)(2,1)}, u32[]{:S(2)}) copy-start(bf16[1,256,1408]{2,1,0:T(8,128)(2,1)} %get-tuple-element.9) | copy-start | bytes 2162692
  112.3 4.7 %copy-start.5 = (bf16[1,256,1408]{2,1,0:T(8,128)(2,1)S(1)}, bf16[1,256,1408]{2,1,0:T(8,128)(2,1)}, u32[]{:S(2)}) copy-start(bf16[1,256,1408]{2,1,0:T(8,128)(2,1)} %get-tuple-element.11) | copy-start | bytes 2162692
  112.3 5.0 %copy-start.6 = (bf16[1,1408,256]{2,1,0:T(8,128)(2,1)S(1)}, bf16[1,1408,256]{2,1,0:T(8,128)(2,1)}, u32[]{:S(2)}) copy-start(bf16[1,1408,256]{2,1,0:T(8,128)(2,1)} %get-tuple-element.13) | copy-start | bytes 2162692
  112.3 17.1 %all-to-all-start.4 = ((bf16[4,192,704]{2,1,0:T(8,128)(2,1)}), bf16[4,192,704]{2,1,0:T(8,128)(2,1)}, u32[]{:S(2)}, u32[]{:S(2)}) async-start(bf16[4,192,704]{2,1,0:T(8,128)(2,1)} %broadcast_in_dim.17), calls=%async_computation.4 | async-start | bytes 2359296 | tf_op jit(solution)/shard_map/all_to_all | solution.py:14
  129.4 25.9 %all-to-all-start.7 = ((bf16[4,3,352,256]{3,2,1,0:T(8,128)(2,1)}), bf16[4,3,352,256]{3,2,1,0:T(8,128)(2,1)S(1)}, u32[]{:S(2)}, u32[]{:S(2)}) async-start(bf16[4,3,352,256]{3,2,1,0:T(8,128)(2,1)} %copy.34), calls=%async_computation.7 | async-start | bytes 4325376 | tf_op jit(solution)/shard_map/all_to_all | solution.py:14
  137.4 22.4 %copy-start.7 = (f32[2,256]{1,0:T(2,128)S(1)}, f32[2,256]{1,0:T(2,128)}, u32[]{:S(2)}) copy-start(f32[2,256]{1,0:T(2,128)} %param.10) | copy-start | bytes 6148
  137.4 22.4 %copy-start.8 = (f32[2,256]{1,0:T(2,128)S(1)}, f32[2,256]{1,0:T(2,128)}, u32[]{:S(2)}) copy-start(f32[2,256]{1,0:T(2,128)} %param.11) | copy-start | bytes 6148
  155.3 33.2 %all-to-all-start.5 = ((bf16[16,48,1024]{2,1,0:T(8,128)(2,1)}), bf16[16,48,1024]{2,1,0:T(8,128)(2,1)}, u32[]{:S(2)}, u32[]{:S(2)}) async-start(bf16[16,48,1024]{2,1,0:T(8,128)(2,1)} %bitcast.95), calls=%async_computation.5 | async-start | bytes 3145728 | tf_op jit(solution)/shard_map/all_to_all | solution.py:14
  180.3 27.3 %collective-permute-start.1 = (bf16[3,352,1024]{2,1,0:T(8,128)(2,1)}, bf16[3,352,1024]{2,1,0:T(8,128)(2,1)S(1)}, u32[]{:S(2)}, u32[]{:S(2)}) collective-permute-start(bf16[3,352,1024]{2,1,0:T(8,128)(2,1)} %bitcast.59), channel_id=1, source_target_pairs={{0,1},{1,0},{2,3},{3,2},{4,5},{5,4},{6,7},{7,6},{8,9},{9,8},{10,11... | collective-permute-start | bytes 6488072 | tf_op jit(solution)/shard_map/ppermute | solution.py:22
  200.7 25.6 %all-to-all-start.6 = ((bf16[16,48,1024]{2,1,0:T(8,128)(2,1)}), bf16[16,48,1024]{2,1,0:T(8,128)(2,1)}, u32[]{:S(2)}, u32[]{:S(2)}) async-start(bf16[16,48,1024]{2,1,0:T(8,128)(2,1)} %broadcast_in_dim.18), calls=%async_computation.6 | async-start | bytes 3145728 | tf_op jit(solution)/shard_map/all_to_all | solution.py:14
  207.7 2.0 copy-start.3
  279.2 29.2 %all-to-all-start.10 = ((bf16[16,192,256]{2,1,0:T(8,128)(2,1)}), bf16[16,192,256]{2,1,0:T(8,128)(2,1)S(1)}, u32[]{:S(2)}, u32[]{:S(2)}) async-start(bf16[16,192,256]{2,1,0:T(8,128)(2,1)} %bitcast.84), calls=%async_computation.10 | async-start | bytes 3145728 | tf_op jit(solution)/shard_map/all_to_all | solution.py:14
  308.4 37.8 %copy-start.1 = (bf16[1536,256]{1,0:T(8,128)(2,1)S(1)}, bf16[1536,256]{1,0:T(8,128)(2,1)}, u32[]{:S(2)}) copy-start(bf16[1536,256]{1,0:T(8,128)(2,1)} %param.6) | copy-start | bytes 2359300
  336.4 8.7 %collective-permute-start.2 = (bf16[768,256]{1,0:T(8,128)(2,1)S(1)}, bf16[768,256]{1,0:T(8,128)(2,1)S(1)}, u32[]{:S(2)}, u32[]{:S(2)}) collective-permute-start(bf16[768,256]{1,0:T(8,128)(2,1)S(1)} %bitcast.97), channel_id=1, source_target_pairs={{0,1},{1,0},{2,3},{3,2},{4,5},{5,4},{6,7},{7,6},{8,9},{9,8},{10,11... | collective-permute-start | bytes 1179656 | tf_op jit(solution)/shard_map/ppermute | solution.py:22
